TPU v7x, 32 devices: a whole 2x2x4 slice. The times are simulated.
32 devices in a mesh: fs: 8 (over z, y), tp: 4 (over x, core).
Axes of the slice: x: 2, y: 2, z: 4, core: 2. Of those that a mesh axis runs over, the one named last changes fastest.
Arguments:
- rnn_out: bfloat16 [6144, 1536], P('fs', 'tp'), may hold values from -6 to 6
- out_grad: bfloat16 [6144, 2048], P('fs', 'tp'), may hold values from -0.109375 to 0.109375
- weight: float32 [2048, 1536], P('fs', 'tp'), may hold values from -0.15625 to 0.15625
- left_root: bfloat16 [4, 2048, 2048], P('tp', 'fs'), as said below
- right_root: bfloat16 [4, 384, 384], P('tp'), as said below
- left_stat: float32 [4, 2048, 2048], P('tp', 'fs'), may hold values from -4 to 4
- right_stat: float32 [4, 384, 384], P('tp', 'fs'), may hold values from -4 to 4
Outputs:
- new_weight: float32 [2048, 1536], P('fs', 'tp')
- step: float32 [2048, 1536], P('fs', 'tp')
- left_new: float32 [4, 2048, 2048], P('tp', 'fs')
- right_new: float32 [4, 384, 384], P('tp', 'fs')
- weight_copy: bfloat16 [2048, 1536], P(None, 'tp')
Inputs may be any that keep to these rules, and one draw needn't show every extreme that they name: `left_root`: each block is symmetric. `right_root`: each block is symmetric.
All inputs are finite; a program needn't handle non-finite values.
Results may differ from a plain program's by a relative error of at most 0.0049.
Values may be sent and summed in bfloat16 or wider, within the bound.
A program may use at most 64 MiB of HBM per device.

v0:
```python
import jax
import jax.numpy as jnp
from jax import lax
from jax.sharding import PartitionSpec as P

decay_rate = 0.8
step_size = 0.005


def body(rnn_out, out_grad, weight, left_root, right_root, left_stat, right_stat):
    block = weight.shape[1]
    width = left_root.shape[2]
    right_rows = right_stat.shape[1]
    right_start = lax.axis_index("fs") * right_rows
    cotangent = lax.all_gather(out_grad, "tp", axis=1, tiled=True)
    grad = lax.psum_scatter(
        lax.dot_general(
            cotangent, rnn_out, (((0,), (0,)), ((), ())), preferred_element_type=jnp.float32
        ),
        "fs",
        scatter_dimension=0,
        tiled=True,
    )
    grad_low = grad.astype(jnp.bfloat16)
    piece = lax.all_gather(grad_low, "fs", axis=0, tiled=True)
    root_columns = left_root[0]
    left_sum = jnp.dot(root_columns, piece, preferred_element_type=jnp.float32)
    own_columns = lax.dynamic_slice_in_dim(piece, right_start, right_rows, 1)
    right_sum = lax.dot_general(
        own_columns, piece, (((0,), (0,)), ((), ())), preferred_element_type=jnp.float32
    )
    product = lax.dot_general(
        grad_low, piece, (((1,), (1,)), ((), ())), preferred_element_type=jnp.float32
    )
    outer = product
    left_sum, right_sum, outer = (left_sum, right_sum, outer)
    grad_square = jnp.sum(grad * grad)
    total_grad = lax.psum(grad_square, ("fs", "tp"))
    left_new = decay_rate * left_stat + (1.0 - decay_rate) * (outer / block)[None]
    right_new = decay_rate * right_stat + (1.0 - decay_rate) * (right_sum / width)[None]
    applied = left_sum.astype(jnp.bfloat16)
    update = jnp.dot(applied, right_root[0], preferred_element_type=jnp.float32)
    update_square = jnp.sum(update * update)
    total_update = lax.psum(update_square, ("fs", "tp"))
    scale = jnp.sqrt(total_grad + 1.0) / jnp.sqrt(total_update + 1.0)
    step = scale * update
    new_weight = weight - step_size * step
    weight_copy = lax.all_gather(new_weight.astype(jnp.bfloat16), "fs", axis=0, tiled=True)
    return (new_weight, step, left_new, right_new, weight_copy)


def solution(mesh):
    placed = (
        P("fs", "tp"),
        P("fs", "tp"),
        P("fs", "tp"),
        P("tp", "fs", None),
        P("tp", None, None),
        P("tp", "fs", None),
        P("tp", "fs", None),
    )
    return jax.shard_map(
        body,
        mesh=mesh,
        in_specs=placed,
        out_specs=(
            P("fs", "tp"),
            P("fs", "tp"),
            P("tp", "fs", None),
            P("tp", "fs", None),
            P(None, "tp"),
        ),
        check_vma=False,
    )
```

profile of v0, /device:TPU:0, one launch (start us, length us, event | category | flops | bytes accessed | tf_op | source)
XLA Modules:
  0.0 267.6 jit_solution(12664198231551516775)
XLA Ops:
  7.2 0.0 copy-start
  7.2 0.0 all-gather.4.cloned.1.call-start
  7.2 0.7 all-gather.4.cloned.1.call-update
  7.9 0.0 reduce-scatter.2.cloned.1.call-start
  8.0 32.9 %all-gather.4.cloned.1.call-done = bf16[768,2048]{1,0:T(8,128)(2,1)} async-done(((bf16[768,512]{1,0:T(8,128)(2,1)}), bf16[768,2048]{1,0:T(8,128)(2,1)}) %all-gather.4.cloned.1.call-update) | async-done | bytes 3145744 | tf_op jit(solution)/shard_map/all_gather | solution.py:15
  40.8 5.5 %fusion.13 = f32[2048,384]{1,0:T(8,128)} fusion(bf16[768,2048]{1,0:T(8,128)(2,1)} %all-gather.4.cloned.1.call-done, bf16[768,384]{1,0:T(8,128)(2,1)} %param.7), kind=kOutput, calls=%fused_computation.17 | convolution fusion | flops 1207959552 | bytes 6881280 | tf_op jit(solution)/shard_map/dot_general | solution.py:17
  46.3 0.0 reduce-scatter.2.cloned.1.call-update
  46.3 0.0 copy-start.3
  46.3 0.0 all-gather.6.cloned.1.call-start
  46.4 74.4 %reduce-scatter.2.cloned.1.call-done = f32[256,384]{1,0:T(8,128)} async-done(((f32[2048,384]{1,0:T(8,128)}), f32[256,384]{1,0:T(8,128)}) %reduce-scatter.2.cloned.1.call-update) | async-done | bytes 393232 | tf_op jit(solution)/shard_map/reduce_scatter | solution.py:16
  120.8 2.4 multiply_reduce_fusion.1
  123.2 0.0 all-gather.6.cloned.1.call-update
  123.3 0.0 copy-start.4
  123.3 0.0 all-gather.8.cloned.1.call-start
  123.3 43.6 %all-gather.6.cloned.1.call-done = bf16[2048,384]{1,0:T(8,128)(2,1)} async-done(((bf16[256,384]{1,0:T(8,128)(2,1)}), bf16[2048,384]{1,0:T(8,128)(2,1)}) %all-gather.6.cloned.1.call-update) | async-done | bytes 1572880 | tf_op jit(solution)/shard_map/all_gather | solution.py:25
  166.9 0.0 copy-done
  166.9 0.0 copy-start.1
  166.9 4.0 %multiply_reduce_fusion = (f32[]{:T(128)}, f32[256,384]{1,0:T(8,128)}) fusion(bf16[1,384,384]{2,1,0:T(8,128)(2,1)} %param.11, bf16[2048,384]{1,0:T(8,128)(2,1)} %all-gather.6.cloned.1.call-done, bf16[1,256,2048]{2,1,0:T(8,128)(2,1)S(1)} %copy-done), kind=kOutput, calls=%fused_computation.11 | convolution fusion | flops 478445568 | bytes 3309572 | tf_op jit(solution)/shard_map/dot_general | solution.py:42
  170.9 0.0 copy-start.2
  170.9 39.4 %all-reduce = (f32[]{:T(128)}, f32[]{:T(128)}) all-reduce(f32[]{:T(128)} %get-tuple-element.10, f32[]{:T(128)} %get-tuple-element.12), channel_id=1, replica_groups=mesh['fs'=8,'tp'=4] {'fs','tp'}, use_global_device_ids=true, to_apply=%region_2.0 | all-reduce | flops 2 | bytes 16 | tf_op jit(solution)/shard_map/psum | solution.py:38
  211.7 0.0 copy-done.3
  211.7 2.0 fusion.10
  213.7 0.0 all-gather.8.cloned.1.call-update
  213.7 0.0 copy-done.4
  213.7 0.0 copy-done.1
  213.7 1.2 fusion.4
  214.9 0.0 copy-done.2
  214.9 3.7 %fusion.1 = f32[1,256,2048]{2,1,0:T(8,128)} fusion(bf16[256,384]{1,0:T(8,128)(2,1)S(1)} %copy-done.2, bf16[2048,384]{1,0:T(8,128)(2,1)S(1)} %copy-done.1, f32[1,256,2048]{2,1,0:T(8,128)} %param.12), kind=kOutput, calls=%fused_computation.2 | convolution fusion | flops 404226048 | bytes 5963776 | tf_op jit(solution)/shard_map/dot_general | solution.py:32
  218.6 39.8 %all-gather.8.cloned.1.call-done = bf16[2048,384]{1,0:T(8,128)(2,1)} async-done(((bf16[256,384]{1,0:T(8,128)(2,1)}), bf16[2048,384]{1,0:T(8,128)(2,1)}) %all-gather.8.cloned.1.call-update) | async-done | bytes 1572880 | tf_op jit(solution)/shard_map/all_gather | solution.py:48
  258.4 2.7 %copy.13 = bf16[2048,384]{1,0:T(8,128)(2,1)} copy(bf16[2048,384]{1,0:T(8,128)(2,1)} %all-gather.8.cloned.1.call-done) | data formatting | bytes 3145728
Async XLA Ops:
  7.2 159.7 %copy-start = (bf16[1,256,2048]{2,1,0:T(8,128)(2,1)S(1)}, bf16[1,256,2048]{2,1,0:T(8,128)(2,1)}, u32[]{:S(2)}) copy-start(bf16[1,256,2048]{2,1,0:T(8,128)(2,1)} %param.10) | copy-start | bytes 3145732
  7.2 33.6 %all-gather.4.cloned.1.call-start = ((), (), s32[]{:S(2)}) async-start(), calls=%async_computation.1 | async-start | bytes 3932160 | tf_op jit(solution)/shard_map/all_gather | solution.py:15
  7.9 112.9 %reduce-scatter.2.cloned.1.call-start = ((), (), s32[]{:S(2)}) async-start(), calls=%async_computation.2 | async-start | bytes 3538944 | tf_op jit(solution)/shard_map/reduce_scatter | solution.py:16
  46.3 165.3 %copy-start.3 = (f32[256,384]{1,0:T(8,128)S(1)}, f32[256,384]{1,0:T(8,128)}, u32[]{:S(2)}) copy-start(f32[256,384]{1,0:T(8,128)} %param.9) | copy-start | bytes 1179652
  46.3 120.6 %all-gather.6.cloned.1.call-start = ((), (), s32[]{:S(2)}) async-start(), calls=%async_computation.3 | async-start | bytes 1769472 | tf_op jit(solution)/shard_map/all_gather | solution.py:25
  123.3 90.4 %copy-start.4 = (f32[1,48,384]{2,1,0:T(8,128)S(1)}, f32[1,48,384]{2,1,0:T(8,128)}, u32[]{:S(2)}) copy-start(f32[1,48,384]{2,1,0:T(8,128)} %param.13) | copy-start | bytes 221188
  123.3 135.1 %all-gather.8.cloned.1.call-start = ((), (), s32[]{:S(2)}) async-start(), calls=%async_computation.4 | async-start | bytes 1769472 | tf_op jit(solution)/shard_map/all_gather | solution.py:48
  166.9 46.8 %copy-start.1 = (bf16[2048,384]{1,0:T(8,128)(2,1)S(1)}, bf16[2048,384]{1,0:T(8,128)(2,1)}, u32[]{:S(2)}) copy-start(bf16[2048,384]{1,0:T(8,128)(2,1)} %all-gather.6.cloned.1.call-done) | copy-start | bytes 4718596
  170.9 44.0 %copy-start.2 = (bf16[256,384]{1,0:T(8,128)(2,1)S(1)}, bf16[256,384]{1,0:T(8,128)(2,1)}, u32[]{:S(2)}) copy-start(bf16[256,384]{1,0:T(8,128)(2,1)} %get-tuple-element.11) | copy-start | bytes 589828
Sparse Core Ops, SparseCore 0:
  9.6 31.2 all-gather.3
  46.4 74.3 reduce-scatter.1
  123.6 43.2 all-gather.5
  213.8 44.5 all-gather.7
where the time goes:
time: 268 us
  waiting for transfers between devices  191 us (71%)
  blocking collectives  39.4 us (15%)
  between operations  15.2 us (6%)
  matrix products  14.4 us (5%)
  other arithmetic  4.42 us (2%)
  local copies, waits for them, and re-layouts  2.74 us (1%)
    reduce_scatter x1, waiting for transfers between devices, body(): lax.psum_scatter(lax.dot_general(cotangent, rnn_out, (((0,), (0,)), ((),...  74.4 us
    all_gather x1, waiting for transfers between devices, body(): piece = lax.all_gather(grad_low, 'fs', axis=0, tiled=True)  43.6 us
    all_gather x1, waiting for transfers between devices, body(): lax.all_gather(new_weight.astype(jnp.bfloat16), 'fs', axis=0, tiled=True)  39.8 us
    psum x1, blocking collectives, body(): total_grad = lax.psum(grad_square, ('fs', 'tp'))  39.4 us
    all_gather x1, waiting for transfers between devices, body(): cotangent = lax.all_gather(out_grad, 'tp', axis=1, tiled=True)  32.9 us
    dot_general x1, matrix products, body(): lax.dot_general(cotangent, rnn_out, (((0,), (0,)), ((), ())), preferred_e...  5.49 us
  transfers between devices with their start and end apart: 4, of which 4 were waited for; matrix products, arithmetic and copies ran while one was open for 2% of the time, Pallas kernels for 0%

commit v1 on v0

--- a/solution.py
+++ b/solution.py
@@ -1,6 +1,10 @@
+import functools
+
 import jax
 import jax.numpy as jnp
 from jax import lax
+from jax.experimental import pallas as pl
+from jax.experimental.pallas import tpu as pltpu
 from jax.sharding import PartitionSpec as P
 
 decay_rate = 0.8
@@ -48,6 +52,303 @@
     weight_copy = lax.all_gather(new_weight.astype(jnp.bfloat16), "fs", axis=0, tiled=True)
     return (new_weight, step, left_new, right_new, weight_copy)
 
+MESH = pl.DeviceIdType.MESH
+HALVES = 2
+
+
+def dot(a, b, contract):
+    return lax.dot_general(a, b, ((contract[:1], contract[1:]), ((), ())), preferred_element_type=jnp.float32)
+
+
+def kernel(nf, nt, rnn, own, weight, root_hbm, right_root, stat_hbm, right_stat,
+           new_weight, step, left_hbm, right_new, copy_out,
+           root, stat, left, from_x, from_core, forwarded, pair_send, pair_recv, kept,
+           line_send, line_recv, total, piece, applied_sum, inner, sums,
+           local_sem, ax_s, ax_r, ac_s, ac_r, af_s, af_r, py_s, py_r, pz_s, pz_r,
+           gz_s, gz_r, gy_s, gy_r, wz_s, wz_r, wy_s, wy_r, s_s, s_r):
+    ny = 2
+    nz = nf // ny
+    count = nf * nt
+    rows, block = weight.shape
+    width = root.shape[1]
+    half = rows // HALVES
+    f, t = lax.axis_index("fs"), lax.axis_index("tp")
+    me = f * nt + t
+    z, y = f // ny, f % ny
+    x, core = t // 2, t % 2
+    other_y = 1 - y
+    partner = {"fs": z * ny + other_y, "tp": t}
+    over_x = {"fs": f, "tp": (1 - x) * 2 + core}
+    over_core = {"fs": f, "tp": x * 2 + 1 - core}
+
+    def remote(src, dst, send, recv, device):
+        return pltpu.make_async_remote_copy(
+            src_ref=src, dst_ref=dst, send_sem=send, recv_sem=recv, device_id=device, device_id_type=MESH
+        )
+
+    def peer(k):
+        flat = (me + k) % count
+        return {"fs": flat // nt, "tp": flat % nt}
+
+    load_root = pltpu.make_async_copy(root_hbm, root, local_sem.at[0])
+    load_stat = pltpu.make_async_copy(stat_hbm, stat, local_sem.at[1])
+    load_root.start()
+    load_stat.start()
+
+    barrier = pltpu.get_barrier_semaphore()
+
+    def greet(k, carry):
+        pl.semaphore_signal(barrier, inc=1, device_id=peer(k), device_id_type=MESH)
+        return carry
+
+    lax.fori_loop(1, count, greet, 0)
+    pl.semaphore_wait(barrier, count - 1)
+
+    def own_chunk(k):
+        c = other_y if k == 0 else y
+        return own.at[:, pl.ds(pl.multiple_of(c * rows, rows), rows)]
+
+    x_copies, core_copies, forward_copies, pair_copies = [], [], [], []
+    for k in range(2):
+        x_copies.append(remote(own_chunk(k), from_x.at[k], ax_s.at[k], ax_r.at[k], over_x))
+        core_copies.append(remote(own_chunk(k), from_core.at[k], ac_s.at[k], ac_r.at[k], over_core))
+        forward_copies.append(remote(from_x.at[k], forwarded.at[k], af_s.at[k], af_r.at[k], over_core))
+    for k in range(2):
+        x_copies[k].start()
+        core_copies[k].start()
+    for s in range(nt):
+        pair_copies.append(remote(pair_send.at[s], pair_recv.at[s], py_s.at[s], py_r.at[s], partner))
+
+    owners = [t, x * 2 + 1 - core, (1 - x) * 2 + core, (1 - x) * 2 + 1 - core]
+
+    def line_copy(s):
+        slot = (owners[s] - z + nz) % nz - 1
+        return remote(line_send.at[s], line_recv.at[slot], pz_s.at[s], pz_r.at[slot],
+                      {"fs": owners[s] * ny + y, "tp": t})
+
+    def multiply(s, k, chunk):
+        product = dot(chunk[...], rnn[...], (0, 0))
+        if k == 0:
+            pair_send[s] = product.astype(jnp.bfloat16)
+            pair_copies[s].start()
+        else:
+            kept[s] = product
+
+    def combine(s):
+        pair_copies[s].wait_recv()
+        both = kept[s] + pair_recv[s].astype(jnp.float32)
+
+        @pl.when(owners[s] == z)
+        def _():
+            total[...] = both
+
+        @pl.when(owners[s] != z)
+        def _():
+            line_send[s] = both.astype(jnp.bfloat16)
+            line_copy(s).start()
+
+    for k in range(2):
+        multiply(0, k, own_chunk(k))
+    for k in range(2):
+        core_copies[k].wait_recv()
+        multiply(1, k, from_core.at[k])
+    combine(0)
+    for k in range(2):
+        x_copies[k].wait_recv()
+        forward_copies[k].start()
+        multiply(2, k, from_x.at[k])
+        if k == 0:
+            combine(1)
+    for k in range(2):
+        forward_copies[k].wait_recv()
+        multiply(3, k, forwarded.at[k])
+        if k == 0:
+            combine(2)
+    combine(3)
+
+    def line_arrival(dz):
+        return remote(line_send.at[0], line_recv.at[dz - 1], pz_s.at[0], pz_r.at[dz - 1], partner)
+
+    for dz in range(1, nz):
+        line_arrival(dz).wait_recv()
+        total[...] += line_recv[dz - 1].astype(jnp.float32)
+    grad = total[...]
+    sums[me, 0:8, :] = jnp.full((8, 128), jnp.sum(grad * grad))
+    piece[f] = grad.astype(jnp.bfloat16)
+
+    def gather(buffer, z_s, z_r, y_s, y_r, use):
+        def part(owner, h):
+            return buffer.at[owner, pl.ds(h * half, half)]
+
+        def along(dz, h):
+            return remote(part(f, h), part(f, h), z_s.at[dz - 1, h], z_r.at[dz - 1, h],
+                          {"fs": (z + dz) % nz * ny + y, "tp": t})
+
+        def source(dz, side):
+            return (z - dz + nz) % nz * ny + side
+
+        def arrival(dz, h):
+            mine = part(source(dz, y), h)
+            return remote(mine, mine, z_s.at[dz - 1, h], z_r.at[dz - 1, h], partner)
+
+        def across(dz, h):
+            mine = part(source(dz, y), h)
+            return remote(mine, mine, y_s.at[dz, h], y_r.at[dz, h], partner)
+
+        def crossed(dz, h):
+            theirs = part(source(dz, other_y), h)
+            return remote(theirs, theirs, y_s.at[dz, h], y_r.at[dz, h], partner)
+
+        for dz in range(1, nz):
+            for h in range(HALVES):
+                along(dz, h).start()
+                if dz == 1:
+                    across(0, h).start()
+        use(f)
+        for dz in range(1, nz):
+            for h in range(HALVES):
+                arrival(dz, h).wait_recv()
+                across(dz, h).start()
+            use(source(dz, y))
+            for h in range(HALVES):
+                crossed(dz - 1, h).wait_recv()
+            use(source(dz - 1, other_y))
+        for h in range(HALVES):
+            crossed(nz - 1, h).wait_recv()
+        use(source(nz - 1, other_y))
+        for dz in range(1, nz):
+            for h in range(HALVES):
+                along(dz, h).wait_send()
+        for dz in range(nz):
+            for h in range(HALVES):
+                across(dz, h).wait_send()
+
+    def columns(owner):
+        return pl.ds(pl.multiple_of(owner * rows, rows), rows)
+
+    load_root.wait()
+    load_stat.wait()
+    applied_sum[...] = jnp.zeros_like(applied_sum)
+
+    def apply_left(owner):
+        applied_sum[...] += dot(root[:, columns(owner)], piece[owner], (1, 0))
+
+    gather(piece, gz_s, gz_r, gy_s, gy_r, apply_left)
+
+    update = dot(applied_sum[...].astype(jnp.bfloat16), right_root[...], (1, 0))
+    step[...] = update
+    sums[me, 8:16, :] = jnp.full((8, 128), jnp.sum(update * update))
+
+    def sum_copy(k):
+        return remote(sums.at[me], sums.at[me], s_s.at[k], s_r.at[k], peer(k))
+
+    def sum_arrival(k):
+        theirs = sums.at[(me - k + count) % count]
+        return remote(theirs, theirs, s_s.at[k], s_r.at[k], peer(k))
+
+    def send_sum(k, carry):
+        sum_copy(k).start()
+        return carry
+
+    def take_sum(k, carry):
+        sum_arrival(k).wait_recv()
+        return carry
+
+    def end_sum(k, carry):
+        sum_copy(k).wait_send()
+        return carry
+
+    lax.fori_loop(1, count, send_sum, 0)
+    inner[...] = jnp.zeros_like(inner)
+    for owner in range(nf):
+        inner[...] += dot(piece[owner], piece[owner], (0, 0))
+    lax.fori_loop(1, count, take_sum, 0)
+    everything = jnp.sum(sums[...], axis=0)
+    scale = jnp.sqrt(everything[0:1, 0:1] + 1.0) / jnp.sqrt(everything[8:9, 0:1] + 1.0)
+    scaled = scale * step[...]
+    step[...] = scaled
+    fresh = weight[...] - step_size * scaled
+    new_weight[...] = fresh
+    copy_out[f] = fresh.astype(jnp.bfloat16)
+
+    def left_block(owner):
+        product = dot(piece[f], piece[owner], (1, 1))
+        left[:, columns(owner)] = decay_rate * stat[:, columns(owner)] + (1.0 - decay_rate) * (product / block)
+
+    gather(copy_out, wz_s, wz_r, wy_s, wy_r, left_block)
+    store_left = pltpu.make_async_copy(left, left_hbm, local_sem.at[2])
+    store_left.start()
+    right_rows = right_stat.shape[0]
+    inner_rows = inner[pl.ds(pl.multiple_of(f * right_rows, 8), right_rows), :]
+    right_new[...] = decay_rate * right_stat[...] + (1.0 - decay_rate) * (inner_rows / width)
+
+    lax.fori_loop(1, count, end_sum, 0)
+    for k in range(2):
+        x_copies[k].wait_send()
+        core_copies[k].wait_send()
+        forward_copies[k].wait_send()
+    for s in range(nt):
+        pair_copies[s].wait_send()
+
+        @pl.when(owners[s] != z)
+        def _():
+            line_copy(s).wait_send()
+
+    store_left.wait()
+
+
+def kernel_body(nf, nt, rnn_out, out_grad, weight, left_root, right_root, left_stat, right_stat):
+    rows, block = weight.shape
+    tokens = rnn_out.shape[0]
+    width = left_root.shape[2]
+    right_rows = right_stat.shape[1]
+    nz = nf // 2
+    low, full = jnp.bfloat16, jnp.float32
+    vmem = pl.BlockSpec(memory_space=pltpu.VMEM)
+    hbm = pl.BlockSpec(memory_space=pl.ANY)
+    dma = pltpu.SemaphoreType.DMA
+    out = pl.pallas_call(
+        functools.partial(kernel, nf, nt),
+        out_shape=(
+            jax.ShapeDtypeStruct((rows, block), full),
+            jax.ShapeDtypeStruct((rows, block), full),
+            jax.ShapeDtypeStruct((rows, width), full),
+            jax.ShapeDtypeStruct((right_rows, block), full),
+            jax.ShapeDtypeStruct((nf, rows, block), low),
+        ),
+        in_specs=[vmem, vmem, vmem, hbm, vmem, hbm, vmem],
+        out_specs=(vmem, vmem, hbm, vmem, vmem),
+        scratch_shapes=[
+            pltpu.VMEM((rows, width), low),
+            pltpu.VMEM((rows, width), full),
+            pltpu.VMEM((rows, width), full),
+            pltpu.VMEM((2, tokens, rows), low),
+            pltpu.VMEM((2, tokens, rows), low),
+            pltpu.VMEM((2, tokens, rows), low),
+            pltpu.VMEM((nt, rows, block), low),
+            pltpu.VMEM((nt, rows, block), low),
+            pltpu.VMEM((nt, rows, block), full),
+            pltpu.VMEM((nt, rows, block), low),
+            pltpu.VMEM((nz - 1, rows, block), low),
+            pltpu.VMEM((rows, block), full),
+            pltpu.VMEM((nf, rows, block), low),
+            pltpu.VMEM((rows, block), full),
+            pltpu.VMEM((block, block), full),
+            pltpu.VMEM((nf * nt, 16, 128), full),
+            dma((3,)),
+            dma((2,)), dma((2,)), dma((2,)), dma((2,)), dma((2,)), dma((2,)),
+            dma((nt,)), dma((nt,)), dma((nt,)), dma((nz - 1,)),
+            dma((nz - 1, HALVES)), dma((nz - 1, HALVES)), dma((nz, HALVES)), dma((nz, HALVES)),
+            dma((nz - 1, HALVES)), dma((nz - 1, HALVES)), dma((nz, HALVES)), dma((nz, HALVES)),
+            dma((nf * nt,)), dma((nf * nt,)),
+        ],
+        compiler_params=pltpu.CompilerParams(
+            collective_id=0, has_side_effects=True, vmem_limit_bytes=60 * 1024 * 1024
+        ),
+    )(rnn_out, out_grad, weight, left_root[0], right_root[0], left_stat[0], right_stat[0])
+    new_weight, step, left_new, right_new, weight_copy = out
+    return new_weight, step, left_new[None], right_new[None], weight_copy.reshape(width, block)
+
 
 def solution(mesh):
     placed = (
@@ -59,8 +360,10 @@
         P("tp", "fs", None),
         P("tp", "fs", None),
     )
+    nf, nt = mesh.shape["fs"], mesh.shape["tp"]
+    chosen = functools.partial(kernel_body, nf, nt) if nt == 4 and nf == 2 * nt else body
     return jax.shard_map(
-        body,
+        chosen,
         mesh=mesh,
         in_specs=placed,
         out_specs=(

time: 268 us -> 122 us (0.46)
  the two profiles are of different devices: /device:TPU:0 before, /device:TPU:24 now
where the time goes in v1:
time: 122 us
  Pallas kernels  112 us (92%)
  local copies, waits for them, and re-layouts  8.57 us (7%)
    pallas_call x1, Pallas kernels, kernel_body(): pl.pallas_call(functools.partial(kernel, nf, nt), out_shape=(jax.ShapeDty...  112 us
    unnamed x9, local copies, waits for them, and re-layouts  8.57 us

profile of v1, /device:TPU:24, one launch (start us, length us, event | category | flops | bytes accessed | tf_op | source)
XLA Modules:
  0.0 121.5 jit_solution(4856809552980746575)
XLA Ops:
  0.6 112.3 %shard_map.110 = (f32[256,384]{1,0:T(8,128)}, f32[256,384]{1,0:T(8,128)}, f32[256,2048]{1,0:T(8,128)}, f32[48,384]{1,0:T(8,128)}, bf16[8,256,384]{2,1,0:T(8,128)(2,1)}) custom-call(bf16[768,384]{1,0:T(8,128)(2,1)} %rnn.1, bf16[768,512]{1,0:T(8,128)(2,1)} %own.1, f32[256,384]{1,0:T(8,128)} %weight.1, bf16[256,2048]{1,0:T(8,128)(2,1)} %bitcast.10, ...), custom_call_target="tpu_custom_call" | custom-call | tf_op jit(solution)/shard_map/pallas_call | solution.py:310
  113.0 1.8 %copy.17 = f32[256,384]{1,0:T(8,128)} copy(f32[256,384]{1,0:T(8,128)} %get-tuple-element.20) | data formatting | bytes 786432
  114.7 1.8 %copy.18 = f32[256,384]{1,0:T(8,128)} copy(f32[256,384]{1,0:T(8,128)} %get-tuple-element.21) | data formatting | bytes 786432
  116.5 0.0 copy-start.1
  116.5 0.0 copy-start
  116.5 3.3 %copy.19 = f32[1,256,2048]{2,1,0:T(8,128)} copy(f32[1,256,2048]{2,1,0:T(8,128)} %bitcast.8) | data formatting | bytes 4194304
  119.8 0.0 copy-done.1
  119.8 0.6 copy.20
  120.4 0.0 copy-done
  120.4 1.1 copy.21
Async XLA Ops:
  116.5 3.3 %copy-start.1 = (f32[48,384]{1,0:T(8,128)S(1)}, f32[48,384]{1,0:T(8,128)}, u32[]{:S(2)}) copy-start(f32[48,384]{1,0:T(8,128)} %get-tuple-element.13) | copy-start | bytes 221188
  116.5 3.9 %copy-start = (bf16[8,256,384]{2,1,0:T(8,128)(2,1)S(1)}, bf16[8,256,384]{2,1,0:T(8,128)(2,1)}, u32[]{:S(2)}) copy-start(bf16[8,256,384]{2,1,0:T(8,128)(2,1)} %get-tuple-element.14) | copy-start | bytes 4718596

commit v2 on v1

--- a/solution.py
+++ b/solution.py
@@ -53,16 +53,16 @@
     return (new_weight, step, left_new, right_new, weight_copy)
 
 MESH = pl.DeviceIdType.MESH
-HALVES = 2
+HALVES = 4
 
 
 def dot(a, b, contract):
     return lax.dot_general(a, b, ((contract[:1], contract[1:]), ((), ())), preferred_element_type=jnp.float32)
 
 
-def kernel(nf, nt, rnn, own, weight, root_hbm, right_root, stat_hbm, right_stat,
-           new_weight, step, left_hbm, right_new, copy_out,
-           root, stat, left, from_x, from_core, forwarded, pair_send, pair_recv, kept,
+def kernel(nf, nt, rnn_hbm, own_hbm, weight_hbm, root_hbm, right_root_hbm, stat_hbm, right_stat_hbm,
+           new_weight, step, left, right_new, copy_out,
+           rnn, weight, right_root, right_stat, root, stat, chip, far, pair_send, pair_recv, kept,
            line_send, line_recv, total, piece, applied_sum, inner, sums,
            local_sem, ax_s, ax_r, ac_s, ac_r, af_s, af_r, py_s, py_r, pz_s, pz_r,
            gz_s, gz_r, gy_s, gy_r, wz_s, wz_r, wy_s, wy_r, s_s, s_r):
@@ -92,8 +92,22 @@
 
     load_root = pltpu.make_async_copy(root_hbm, root, local_sem.at[0])
     load_stat = pltpu.make_async_copy(stat_hbm, stat, local_sem.at[1])
-    load_root.start()
-    load_stat.start()
+    load_own = []
+    for k in range(2):
+        chunk = pl.ds(pl.multiple_of((other_y if k == 0 else y) * rows, rows), rows)
+        load_own.append(pltpu.make_async_copy(own_hbm.at[:, chunk], chip.at[core, k], local_sem.at[2 + k]))
+        load_own[k].start()
+    load_rnn = pltpu.make_async_copy(rnn_hbm, rnn, local_sem.at[4])
+    later = [
+        load_root,
+        load_stat,
+        pltpu.make_async_copy(weight_hbm, weight, local_sem.at[5]),
+        pltpu.make_async_copy(right_root_hbm, right_root, local_sem.at[6]),
+        pltpu.make_async_copy(right_stat_hbm, right_stat, local_sem.at[7]),
+    ]
+    load_rnn.start()
+    for load in later:
+        load.start()
 
     barrier = pltpu.get_barrier_semaphore()
 
@@ -104,22 +118,36 @@
     lax.fori_loop(1, count, greet, 0)
     pl.semaphore_wait(barrier, count - 1)
 
-    def own_chunk(k):
-        c = other_y if k == 0 else y
-        return own.at[:, pl.ds(pl.multiple_of(c * rows, rows), rows)]
+    tokens = rnn.shape[0]
+    split = tokens // 2
+    share = pl.ds(pl.multiple_of(core * split, split), split)
 
     x_copies, core_copies, forward_copies, pair_copies = [], [], [], []
     for k in range(2):
-        x_copies.append(remote(own_chunk(k), from_x.at[k], ax_s.at[k], ax_r.at[k], over_x))
-        core_copies.append(remote(own_chunk(k), from_core.at[k], ac_s.at[k], ac_r.at[k], over_core))
-        forward_copies.append(remote(from_x.at[k], forwarded.at[k], af_s.at[k], af_r.at[k], over_core))
-    for k in range(2):
-        x_copies[k].start()
+        core_copies.append(remote(chip.at[core, k], chip.at[core, k], ac_s.at[k], ac_r.at[k], over_core))
+    for i in range(4):
+        holder = x if i < 2 else 1 - x
+        mine = far.at[i, share]
+        x_copies.append(remote(chip.at[holder, i % 2, share], mine, ax_s.at[i], ax_r.at[i], over_x))
+        forward_copies.append(remote(mine, mine, af_s.at[i], af_r.at[i], over_core))
+
+    def start_first():
+        for i in range(2):
+            x_copies[i].start()
+
+    for k in range(2):
+        load_own[k].wait()
         core_copies[k].start()
+    pl.when(core == x)(start_first)
+    for k in range(2):
+        core_copies[k].wait_recv()
+    pl.when(core != x)(start_first)
+    for i in range(2, 4):
+        x_copies[i].start()
     for s in range(nt):
         pair_copies.append(remote(pair_send.at[s], pair_recv.at[s], py_s.at[s], py_r.at[s], partner))
 
-    owners = [t, x * 2 + 1 - core, (1 - x) * 2 + core, (1 - x) * 2 + 1 - core]
+    owners = [t, x * 2 + 1 - core, (1 - x) * 2 + 1 - x, (1 - x) * 2 + x]
 
     def line_copy(s):
         slot = (owners[s] - z + nz) % nz - 1
@@ -147,23 +175,20 @@
             line_send[s] = both.astype(jnp.bfloat16)
             line_copy(s).start()
 
-    for k in range(2):
-        multiply(0, k, own_chunk(k))
-    for k in range(2):
-        core_copies[k].wait_recv()
-        multiply(1, k, from_core.at[k])
-    combine(0)
-    for k in range(2):
-        x_copies[k].wait_recv()
-        forward_copies[k].start()
-        multiply(2, k, from_x.at[k])
-        if k == 0:
-            combine(1)
-    for k in range(2):
-        forward_copies[k].wait_recv()
-        multiply(3, k, forwarded.at[k])
-        if k == 0:
-            combine(2)
+    load_rnn.wait()
+    for load in later:
+        load.wait()
+    for k in range(2):
+        multiply(0, k, chip.at[core, k])
+    for k in range(2):
+        multiply(1, k, chip.at[1 - core, k])
+    for i in range(4):
+        x_copies[i].wait_recv()
+        forward_copies[i].start()
+        forward_copies[i].wait_recv()
+        multiply(2 + i // 2, i % 2, far.at[i])
+        if i < 3:
+            combine(i)
     combine(3)
 
     def line_arrival(dz):
@@ -173,61 +198,77 @@
         line_arrival(dz).wait_recv()
         total[...] += line_recv[dz - 1].astype(jnp.float32)
     grad = total[...]
-    sums[me, 0:8, :] = jnp.full((8, 128), jnp.sum(grad * grad))
+    grad_square = jnp.sum(grad * grad)
     piece[f] = grad.astype(jnp.bfloat16)
 
     def gather(buffer, z_s, z_r, y_s, y_r, use):
         def part(owner, h):
             return buffer.at[owner, pl.ds(h * half, half)]
 
-        def along(dz, h):
-            return remote(part(f, h), part(f, h), z_s.at[dz - 1, h], z_r.at[dz - 1, h],
-                          {"fs": (z + dz) % nz * ny + y, "tp": t})
-
-        def source(dz, side):
-            return (z - dz + nz) % nz * ny + side
-
-        def arrival(dz, h):
-            mine = part(source(dz, y), h)
-            return remote(mine, mine, z_s.at[dz - 1, h], z_r.at[dz - 1, h], partner)
-
-        def across(dz, h):
-            mine = part(source(dz, y), h)
-            return remote(mine, mine, y_s.at[dz, h], y_r.at[dz, h], partner)
-
-        def crossed(dz, h):
-            theirs = part(source(dz, other_y), h)
-            return remote(theirs, theirs, y_s.at[dz, h], y_r.at[dz, h], partner)
-
-        for dz in range(1, nz):
+        def block_at(way, d, side):
+            return (z - way * d + nz) % nz * ny + side
+
+        def slot(way, d):
+            return d if way > 0 else nz + d
+
+        def onward(way, d, h):
+            mine = part(block_at(way, d, y), h)
+            there = (z + way + nz) % nz * ny + y
+            return remote(mine, mine, z_s.at[slot(way, d), h], z_r.at[slot(way, d + 1), h], {"fs": there, "tp": t})
+
+        def arrival(way, d, h):
+            mine = part(block_at(way, d, y), h)
+            return remote(mine, mine, z_s.at[slot(way, d), h], z_r.at[slot(way, d), h], partner)
+
+        def across(way, d, h, side):
+            mine = part(block_at(way, d, side), h)
+            return remote(mine, mine, y_s.at[slot(way, d), h], y_r.at[slot(way, d), h], partner)
+
+        def comes(way, d):
+            return z >= d if way > 0 else z + d < nz
+
+        def goes(way):
+            return z + 1 < nz if way > 0 else z >= 1
+
+        for h in range(HALVES):
+            for way in (1, -1):
+                pl.when(goes(way))(onward(way, 0, h).start)
+            across(1, 0, h, y).start()
+        use(f)
+        for d in range(1, nz):
             for h in range(HALVES):
-                along(dz, h).start()
-                if dz == 1:
-                    across(0, h).start()
-        use(f)
-        for dz in range(1, nz):
-            for h in range(HALVES):
-                arrival(dz, h).wait_recv()
-                across(dz, h).start()
-            use(source(dz, y))
-            for h in range(HALVES):
-                crossed(dz - 1, h).wait_recv()
-            use(source(dz - 1, other_y))
-        for h in range(HALVES):
-            crossed(nz - 1, h).wait_recv()
-        use(source(nz - 1, other_y))
-        for dz in range(1, nz):
-            for h in range(HALVES):
-                along(dz, h).wait_send()
-        for dz in range(nz):
-            for h in range(HALVES):
-                across(dz, h).wait_send()
+                for way in (1, -1):
+                    @pl.when(comes(way, d))
+                    def _(way=way, h=h):
+                        arrival(way, d, h).wait_recv()
+                        if d + 1 < nz:
+                            pl.when(goes(way))(onward(way, d, h).start)
+                        across(way, d, h, y).start()
+            for way in (1, -1):
+                @pl.when(comes(way, d))
+                def _(way=way):
+                    use(block_at(way, d, y))
+        for d in range(nz):
+            for way in (1, -1):
+                if d or way > 0:
+                    @pl.when(comes(way, d))
+                    def _(way=way, d=d):
+                        for h in range(HALVES):
+                            across(way, d, h, other_y).wait_recv()
+                        use(block_at(way, d, other_y))
+        for d in range(nz):
+            for way in (1, -1):
+                @pl.when(comes(way, d))
+                def _(way=way, d=d):
+                    for h in range(HALVES):
+                        if d + 1 < nz:
+                            pl.when(goes(way))(onward(way, d, h).wait_send)
+                        if d or way > 0:
+                            across(way, d, h, y).wait_send()
 
     def columns(owner):
         return pl.ds(pl.multiple_of(owner * rows, rows), rows)
 
-    load_root.wait()
-    load_stat.wait()
     applied_sum[...] = jnp.zeros_like(applied_sum)
 
     def apply_left(owner):
@@ -237,7 +278,8 @@
 
     update = dot(applied_sum[...].astype(jnp.bfloat16), right_root[...], (1, 0))
     step[...] = update
-    sums[me, 8:16, :] = jnp.full((8, 128), jnp.sum(update * update))
+    lane = lax.broadcasted_iota(jnp.int32, (1, 128), 1)
+    sums[me] = jnp.where(lane < 64, grad_square, jnp.sum(update * update))
 
     def sum_copy(k):
         return remote(sums.at[me], sums.at[me], s_s.at[k], s_r.at[k], peer(k))
@@ -264,7 +306,7 @@
         inner[...] += dot(piece[owner], piece[owner], (0, 0))
     lax.fori_loop(1, count, take_sum, 0)
     everything = jnp.sum(sums[...], axis=0)
-    scale = jnp.sqrt(everything[0:1, 0:1] + 1.0) / jnp.sqrt(everything[8:9, 0:1] + 1.0)
+    scale = jnp.sqrt(everything[0:1, 0:1] + 1.0) / jnp.sqrt(everything[0:1, 64:65] + 1.0)
     scaled = scale * step[...]
     step[...] = scaled
     fresh = weight[...] - step_size * scaled
@@ -276,17 +318,16 @@
         left[:, columns(owner)] = decay_rate * stat[:, columns(owner)] + (1.0 - decay_rate) * (product / block)
 
     gather(copy_out, wz_s, wz_r, wy_s, wy_r, left_block)
-    store_left = pltpu.make_async_copy(left, left_hbm, local_sem.at[2])
-    store_left.start()
     right_rows = right_stat.shape[0]
     inner_rows = inner[pl.ds(pl.multiple_of(f * right_rows, 8), right_rows), :]
     right_new[...] = decay_rate * right_stat[...] + (1.0 - decay_rate) * (inner_rows / width)
 
     lax.fori_loop(1, count, end_sum, 0)
     for k in range(2):
-        x_copies[k].wait_send()
         core_copies[k].wait_send()
-        forward_copies[k].wait_send()
+    for i in range(4):
+        x_copies[i].wait_send()
+        forward_copies[i].wait_send()
     for s in range(nt):
         pair_copies[s].wait_send()
 
@@ -294,7 +335,30 @@
         def _():
             line_copy(s).wait_send()
 
-    store_left.wait()
+
+def settle_kernel(count, *refs):
+    ins, outs, held, sems = refs[:count], refs[count:2 * count], refs[2 * count:3 * count], refs[3 * count]
+    order = sorted(range(count), key=lambda i: -ins[i].size)
+    for i in order:
+        pltpu.make_async_copy(ins[i], held[i], sems.at[0, i]).start()
+    for i in order[::-1]:
+        pltpu.make_async_copy(ins[i], held[i], sems.at[0, i]).wait()
+        pltpu.make_async_copy(held[i], outs[i], sems.at[1, i]).start()
+    for i in order:
+        pltpu.make_async_copy(held[i], outs[i], sems.at[1, i]).wait()
+
+
+def settle(arrays):
+    count = len(arrays)
+    hbm = pl.BlockSpec(memory_space=pl.ANY)
+    return pl.pallas_call(
+        functools.partial(settle_kernel, count),
+        out_shape=tuple(jax.ShapeDtypeStruct(a.shape, a.dtype) for a in arrays),
+        in_specs=[hbm] * count,
+        out_specs=(hbm,) * count,
+        scratch_shapes=[pltpu.VMEM(a.shape, a.dtype) for a in arrays] + [pltpu.SemaphoreType.DMA((2, count))],
+        compiler_params=pltpu.CompilerParams(vmem_limit_bytes=58 * 1024 * 1024),
+    )(*arrays)
 
 
 def kernel_body(nf, nt, rnn_out, out_grad, weight, left_root, right_root, left_stat, right_stat):
@@ -305,7 +369,7 @@
     nz = nf // 2
     low, full = jnp.bfloat16, jnp.float32
     vmem = pl.BlockSpec(memory_space=pltpu.VMEM)
-    hbm = pl.BlockSpec(memory_space=pl.ANY)
+    hbm = pl.BlockSpec(memory_space=pltpu.HBM)
     dma = pltpu.SemaphoreType.DMA
     out = pl.pallas_call(
         functools.partial(kernel, nf, nt),
@@ -316,15 +380,17 @@
             jax.ShapeDtypeStruct((right_rows, block), full),
             jax.ShapeDtypeStruct((nf, rows, block), low),
         ),
-        in_specs=[vmem, vmem, vmem, hbm, vmem, hbm, vmem],
-        out_specs=(vmem, vmem, hbm, vmem, vmem),
+        in_specs=[hbm] * 7,
+        out_specs=(vmem,) * 5,
         scratch_shapes=[
+            pltpu.VMEM((tokens, block), low),
+            pltpu.VMEM((rows, block), full),
+            pltpu.VMEM((block, block), low),
+            pltpu.VMEM((right_rows, block), full),
             pltpu.VMEM((rows, width), low),
             pltpu.VMEM((rows, width), full),
-            pltpu.VMEM((rows, width), full),
-            pltpu.VMEM((2, tokens, rows), low),
-            pltpu.VMEM((2, tokens, rows), low),
-            pltpu.VMEM((2, tokens, rows), low),
+            pltpu.VMEM((2, 2, tokens, rows), low),
+            pltpu.VMEM((4, tokens, rows), low),
             pltpu.VMEM((nt, rows, block), low),
             pltpu.VMEM((nt, rows, block), low),
             pltpu.VMEM((nt, rows, block), full),
@@ -334,19 +400,19 @@
             pltpu.VMEM((nf, rows, block), low),
             pltpu.VMEM((rows, block), full),
             pltpu.VMEM((block, block), full),
-            pltpu.VMEM((nf * nt, 16, 128), full),
-            dma((3,)),
-            dma((2,)), dma((2,)), dma((2,)), dma((2,)), dma((2,)), dma((2,)),
+            pltpu.VMEM((nf * nt, 1, 128), full),
+            dma((8,)),
+            dma((4,)), dma((4,)), dma((2,)), dma((2,)), dma((4,)), dma((4,)),
             dma((nt,)), dma((nt,)), dma((nt,)), dma((nz - 1,)),
-            dma((nz - 1, HALVES)), dma((nz - 1, HALVES)), dma((nz, HALVES)), dma((nz, HALVES)),
-            dma((nz - 1, HALVES)), dma((nz - 1, HALVES)), dma((nz, HALVES)), dma((nz, HALVES)),
+            dma((2 * nz, HALVES)), dma((2 * nz, HALVES)), dma((2 * nz, HALVES)), dma((2 * nz, HALVES)),
+            dma((2 * nz, HALVES)), dma((2 * nz, HALVES)), dma((2 * nz, HALVES)), dma((2 * nz, HALVES)),
             dma((nf * nt,)), dma((nf * nt,)),
         ],
         compiler_params=pltpu.CompilerParams(
-            collective_id=0, has_side_effects=True, vmem_limit_bytes=60 * 1024 * 1024
+            collective_id=0, has_side_effects=True, vmem_limit_bytes=58 * 1024 * 1024
         ),
     )(rnn_out, out_grad, weight, left_root[0], right_root[0], left_stat[0], right_stat[0])
-    new_weight, step, left_new, right_new, weight_copy = out
+    new_weight, step, left_new, right_new, weight_copy = settle(out)
     return new_weight, step, left_new[None], right_new[None], weight_copy.reshape(width, block)
 
 

time: 122 us -> 97 us (0.80)
  the two profiles are of different devices: /device:TPU:24 before, /device:TPU:0 now
where the time goes in v2:
time: 97 us; the launch traced here: 96.9 us
  Pallas kernels  96.2 us (99%)
    pallas_call x1, Pallas kernels, kernel_body(): pl.pallas_call(functools.partial(kernel, nf, nt), out_shape=(jax.ShapeDty...  91.8 us
    pallas_call x1, Pallas kernels, settle(): pl.pallas_call(functools.partial(settle_kernel, count), out_shape=tuple((...  4.43 us

profile of v2, /device:TPU:0, one launch (start us, length us, event | category | flops | bytes accessed | tf_op | source)
XLA Modules:
  0.0 96.9 jit_solution(14655873735930195051)
XLA Ops:
  0.6 91.8 %shard_map.110 = (f32[256,384]{1,0:T(8,128)}, f32[256,384]{1,0:T(8,128)}, f32[256,2048]{1,0:T(8,128)}, f32[48,384]{1,0:T(8,128)}, bf16[8,256,384]{2,1,0:T(8,128)(2,1)}) custom-call(bf16[768,384]{1,0:T(8,128)(2,1)} %rnn_hbm.1, bf16[768,512]{1,0:T(8,128)(2,1)} %own_hbm.1, f32[256,384]{1,0:T(8,128)} %weight_hbm.1, bf16[256,2048]{1,0:T(8,128)(2,1)} %bitcast.8, ...), custom_call_target="tpu_custom_call" | custom-call | tf_op jit(solution)/shard_map/pallas_call | solution.py:374
  92.4 4.4 %shard_map.111 = (f32[256,384]{1,0:T(8,128)}, f32[256,384]{1,0:T(8,128)}, f32[256,2048]{1,0:T(8,128)}, f32[48,384]{1,0:T(8,128)}, bf16[8,256,384]{2,1,0:T(8,128)(2,1)}) custom-call(f32[256,384]{1,0:T(8,128)} %get-tuple-element.15.refs_0_, f32[256,384]{1,0:T(8,128)} %get-tuple-element.16.refs_1_, f32[256,2048]{1,0:T(8,128)} %get-tuple-element.17.refs_2_, ...), custom_call_target="tpu_custom_call" | custom-call | tf_op jit(solution)/shard_map/pallas_call | solution.py:354
